TPU v7x, 32 devices: a whole 2x2x4 slice. The times are simulated.
32 devices in a mesh: sp: 16 (over z, y, x), tp: 2 (over core).
Axes of the slice: x: 2, y: 2, z: 4, core: 2. Of those that a mesh axis runs over, the one named last changes fastest.
Arguments:
- resid: bfloat16 [4096, 2048], P('sp', 'tp'), may hold values from -6 to 6
- queries: bfloat16 [4096, 1024], P('sp', 'tp'), may hold values from -6 to 6
- keys_values: bfloat16 [8, 4096, 128], P('tp', 'sp'), may hold values from -6 to 6
- cum_gate: float32 [16, 4096], P('tp', 'sp'), as said below
- out_weight: bfloat16 [1024, 2048], P(None, 'tp'), may hold values from -1.5 to 1.5
- norm_gain: float32 [2048], replicated, may hold values from 0.1 to 1.9
- gate_weight: bfloat16 [2048, 5632], P('sp', 'tp'), may hold values from -0.125 to 0.125
- up_weight: bfloat16 [2048, 5632], P('sp', 'tp'), may hold values from -0.125 to 0.125
- conv_kernel: float32 [3, 2, 5632], P(None, None, 'tp'), may hold values from -3.5 to 3.5
- down_weight: bfloat16 [5632, 2048], P('tp', 'sp'), may hold values from -0.078125 to 0.078125
Outputs:
- layer_out: bfloat16 [4096, 2048], P('sp', 'tp')
Inputs may be any that keep to these rules, and one draw needn't show every extreme that they name: `cum_gate`: along positions each head's entries never increase.
All inputs are finite; a program needn't handle non-finite values.
Results may differ from a plain program's by a relative error of at most 0.015.
Values may be sent and summed in bfloat16 or wider, within the bound.
A program may use at most 128 MiB of HBM per device.

v0:
```python
import jax
import jax.numpy as jnp
from jax import lax
from jax.sharding import PartitionSpec as P

norm_eps = 1e-06


def from_behind(value, axis, by):
    size = lax.axis_size(axis)
    pairs = [(i, i + by) for i in range(size) if 0 <= i + by < size]
    return lax.ppermute(value, axis, pairs)


def attend(queries, keys_values, cum_gate, row_start):
    tok_rows = queries.shape[0]
    local_pairs = keys_values.shape[0]
    head_dim = keys_values.shape[2] // 2
    local_heads = cum_gate.shape[0]
    group_size = local_heads // local_pairs
    score_scale = head_dim ** (-0.5)
    query_heads = queries.reshape(tok_rows, local_pairs, group_size, head_dim)
    all_gates = lax.all_gather(cum_gate, "sp", axis=1, tiled=True)
    own_gates = lax.dynamic_slice_in_dim(all_gates, row_start, tok_rows, 1).reshape(
        local_pairs, group_size, tok_rows
    )
    query_pos = row_start + jnp.arange(tok_rows, dtype=jnp.int32)
    last_row = row_start + tok_rows - 1

    def add_block(state_now, key_block, offset):
        block_width = key_block.shape[1]
        key_part = key_block[:, :, :head_dim]
        values = key_block[:, :, head_dim:]
        key_gates = lax.dynamic_slice_in_dim(all_gates, offset, block_width, 1).reshape(
            local_pairs, group_size, block_width
        )
        scores = (
            jnp.einsum("tkgd,krd->kgtr", query_heads, key_part, preferred_element_type=jnp.float32)
            * score_scale
        )
        scores = scores + own_gates[:, :, :, None] - key_gates[:, :, None, :]
        visible = query_pos[:, None] >= (offset + jnp.arange(block_width, dtype=jnp.int32))[None, :]
        scores = jnp.where(visible, scores, -1e30)
        running_max, running_sum, weighted = state_now
        next_max = jnp.maximum(running_max, jnp.max(scores, axis=3))
        weights = jnp.where(visible, jnp.exp(scores - next_max[:, :, :, None]), 0.0)
        shrink = jnp.exp(running_max - next_max)
        running_sum = running_sum * shrink + jnp.sum(weights, axis=3)
        weighted = weighted * shrink[:, :, :, None] + jnp.einsum(
            "kgtr,krd->kgtd",
            weights.astype(jnp.bfloat16),
            values,
            preferred_element_type=jnp.float32,
        )
        return (next_max, running_sum, weighted)

    start_state = (
        jnp.full((local_pairs, group_size, tok_rows), -1e30, jnp.float32),
        jnp.zeros((local_pairs, group_size, tok_rows), jnp.float32),
        jnp.zeros((local_pairs, group_size, tok_rows, head_dim), jnp.float32),
    )
    arrived = lax.all_gather(keys_values, "sp", axis=1, tiled=True)
    arrived_rows = arrived.shape[1]
    block_rows = 512

    def fold_block(block_index, inner):
        block_start = block_index * block_rows
        key_block = lax.dynamic_slice_in_dim(arrived, block_index * block_rows, block_rows, 1)
        return lax.cond(
            block_start <= last_row,
            lambda current: add_block(current, key_block, block_start),
            lambda current: current,
            inner,
        )

    running_max, running_sum, weighted = lax.fori_loop(
        0, arrived_rows // block_rows, fold_block, start_state
    )
    result = (weighted / running_sum[:, :, :, None]).transpose(2, 0, 1, 3)
    return result.reshape(tok_rows, local_heads * head_dim).astype(jnp.bfloat16)


def local(
    resid,
    queries,
    keys_values,
    cum_gate,
    out_weight,
    norm_gain,
    gate_weight,
    up_weight,
    conv_kernel,
    down_weight,
):
    tok_rows = resid.shape[0]
    hidden_cols = gate_weight.shape[1]
    row_start = lax.axis_index("sp") * tok_rows
    attn = attend(queries, keys_values, cum_gate, row_start)
    branch = jnp.dot(
        lax.all_gather(attn, "tp", axis=1, tiled=True),
        out_weight,
        preferred_element_type=jnp.float32,
    )
    middle = (resid.astype(jnp.float32) + branch).astype(jnp.bfloat16)
    middle_f32 = middle.astype(jnp.float32)
    middle_full = lax.all_gather(middle, "tp", axis=1, tiled=True).astype(jnp.float32)
    inverse = lax.rsqrt(jnp.mean(middle_full * middle_full, axis=1, keepdims=True) + norm_eps)
    normed = (middle_full * inverse * norm_gain).astype(jnp.bfloat16)
    gate_sum = jnp.dot(
        normed,
        lax.all_gather(gate_weight, "sp", axis=0, tiled=True),
        preferred_element_type=jnp.float32,
    )
    up_sum = jnp.dot(
        normed,
        lax.all_gather(up_weight, "sp", axis=0, tiled=True),
        preferred_element_type=jnp.float32,
    )
    pre_gate = gate_sum.astype(jnp.bfloat16)
    pre_up = up_sum.astype(jnp.bfloat16)
    reach_back = conv_kernel.shape[0] - 1
    joined = jnp.concatenate([pre_gate, pre_up], axis=1)
    before = from_behind(joined[tok_rows - reach_back :], "sp", 1)
    padded = jnp.concatenate([before, joined], axis=0).astype(jnp.float32)
    kernel = conv_kernel.reshape(reach_back + 1, 2 * hidden_cols)
    mixed = jnp.zeros((tok_rows, 2 * hidden_cols), jnp.float32)
    for offset in range(reach_back + 1):
        mixed = mixed + kernel[offset][None, :] * padded[offset : offset + tok_rows]
    hidden = (jax.nn.silu(mixed[:, :hidden_cols]) * mixed[:, hidden_cols:]).astype(jnp.bfloat16)
    partials = jnp.dot(
        hidden,
        lax.all_gather(down_weight, "sp", axis=1, tiled=True),
        preferred_element_type=jnp.float32,
    )
    channel_out = lax.psum_scatter(
        partials.astype(jnp.bfloat16), "tp", scatter_dimension=1, tiled=True
    ).astype(jnp.float32)
    return (middle_f32 + channel_out).astype(jnp.bfloat16)


def solution(mesh):
    return jax.shard_map(
        local,
        mesh=mesh,
        in_specs=(
            P("sp", "tp"),
            P("sp", "tp"),
            P("tp", "sp", None),
            P("tp", "sp"),
            P(None, "tp"),
            P(),
            P("sp", "tp"),
            P("sp", "tp"),
            P(None, None, "tp"),
            P("tp", "sp"),
        ),
        out_specs=P("sp", "tp"),
        check_vma=False,
    )
```

profile of v0, /device:TPU:0, one launch (start us, length us, event | category | flops | bytes accessed | tf_op | source)
XLA Modules:
  0.0 685.5 jit_solution(4768735813569886703)
XLA Ops:
  6.5 0.0 copy-start
  6.5 0.0 all-gather.6.cloned.1.call-start
  6.5 1.9 copy.12
  8.5 0.0 all-gather.6.cloned.1.call-update
  8.5 0.0 all-gather.8.cloned.1.call-start
  8.6 1.8 copy.13
  10.4 43.6 %all_gather.22 = f32[8,4096]{1,0:T(8,128)S(1)} all-gather(f32[8,256]{1,0:T(8,128)} %param.17), channel_id=1, replica_groups=mesh['sp'=16,'tp'=2] {'sp'}, dimensions={1}, use_global_device_ids=true | all-gather | bytes 139264 | tf_op jit(solution)/shard_map/all_gather | solution.py:23
  54.0 46.1 %all-gather.6.cloned.1.call-done = bf16[4,4096,128]{1,2,0:T(8,128)(2,1)} async-done(((bf16[4,256,128]{1,2,0:T(8,128)(2,1)}), bf16[4,4096,128]{1,2,0:T(8,128)(2,1)}) %all-gather.6.cloned.1.call-update) | async-done | bytes 4194320 | tf_op jit(solution)/shard_map/all_gather | solution.py:62
  100.2 0.0 copy-start.4
  100.2 10.1 %while.18 = (s32[]{:T(128)}, f32[4,2,256]{2,1,0:T(2,128)S(1)}, f32[4,2,256]{2,1,0:T(2,128)S(1)}, f32[4,2,256,64]{2,3,1,0:T(8,128)S(1)}, s32[]{:T(128)}, /*index=...) while((s32[]{:T(128)}, f32[4,2,256]{2,1,0:T(2,128)S(1)}, ...), condition=%wide.region_5.6_spmd.clone, body=%wide.region_0.5_spmd.clone.sunk | while | flops 288756480 | bytes 32014712 | solution.py:76
  100.3 9.7 %conditional.3 = ((f32[4,2,256]{2,1,0:T(2,128)S(1)}, f32[4,2,256]{2,1,0:T(2,128)S(1)}, f32[4,2,256,64]{2,3,1,0:T(8,128)S(1)})) conditional(s32[]{:T(128)} %convert_element_type.103, (f32[4,2,256]{2,1,0:T(2,128)S(1)}, f32[4,2,256]{2,1,0:T(2,128)S(1)}, f32[4,2,256,64]{2,3,1,0:T(8,128)S(1)}) %tuple.53, (s32[]{:T(128)}, s32[]{:T(128)}, ...), branch_computations={%region_1.0_spmd, %region_2.4_spmd} | conditional | flops 288756480 | bytes 32013442 | solution.py:69
  100.3 0.1 broadcast_compare_fusion
  100.5 2.5 fusion.6
  103.0 0.0 copy-start.2
  103.0 2.0 copy-done.2
  105.0 1.5 fusion.5
  106.5 3.4 fusion.10
  110.4 0.0 copy-start.6
  110.4 2.2 all_gather.23
  112.6 0.0 copy-done
  112.6 0.0 copy-done.4
  112.6 1.5 fusion.27
  114.1 0.0 all-gather.8.cloned.1.call-update
  114.1 0.0 all-gather.10.cloned.1.call-start
  114.2 0.7 all-gather.10.cloned.1.call-update
  114.9 0.0 all-gather.12.cloned.1.call-start
  114.9 0.5 all-gather.12.cloned.1.call-update
  115.4 0.0 all-gather.14.cloned.1.call-start
  115.5 0.5 all-gather.14.cloned.1.call-update
  116.0 0.0 reduce-scatter.2.cloned.1.call-start
  116.1 73.0 %all-gather.8.cloned.1.call-done = bf16[256,2048]{1,0:T(8,128)(2,1)} async-done(((bf16[256,1024]{1,0:T(8,128)(2,1)}), bf16[256,2048]{1,0:T(8,128)(2,1)}) %all-gather.8.cloned.1.call-update) | async-done | bytes 1048592 | tf_op jit(solution)/shard_map/all_gather | solution.py:106
  189.1 1.5 fusion.22
  190.6 143.9 %all-gather.10.cloned.1.call-done = bf16[2048,2816]{1,0:T(8,128)(2,1)} async-done(((bf16[128,2816]{1,0:T(8,128)(2,1)}), bf16[2048,2816]{1,0:T(8,128)(2,1)}) %all-gather.10.cloned.1.call-update) | async-done | bytes 11534352 | tf_op jit(solution)/shard_map/all_gather | solution.py:111
  334.5 7.8 %convolution_convert_fusion.1 = bf16[256,2816]{1,0:T(8,128)(2,1)S(1)} fusion(bf16[2048,2816]{1,0:T(8,128)(2,1)} %all-gather.10.cloned.1.call-done, bf16[256,2048]{1,0:T(8,128)(2,1)} %all-gather.8.cloned.1.call-done, f32[2048]{0:T(1024)S(1)} %copy-done.6, f32[256]{0:T(256)S(1)} %add_rsqrt_fusion), kind=kOutput, calls=%fused_computation.31 | convolution fusion | flops 2955608064 | bytes 14033920 | tf_op jit(solution)/shard_map/dot_general | solution.py:109
  342.3 0.0 copy-start.5
  342.3 134.4 %all-gather.12.cloned.1.call-done = bf16[2048,2816]{1,0:T(8,128)(2,1)} async-done(((bf16[128,2816]{1,0:T(8,128)(2,1)}), bf16[2048,2816]{1,0:T(8,128)(2,1)}) %all-gather.12.cloned.1.call-update) | async-done | bytes 11534352 | tf_op jit(solution)/shard_map/all_gather | solution.py:116
  476.7 7.8 %convolution_convert_fusion = bf16[256,2816]{1,0:T(8,128)(2,1)S(1)} fusion(bf16[2048,2816]{1,0:T(8,128)(2,1)} %all-gather.12.cloned.1.call-done, bf16[256,2048]{1,0:T(8,128)(2,1)} %all-gather.8.cloned.1.call-done, f32[2048]{0:T(1024)S(1)} %copy-done.6, f32[256]{0:T(256)S(1)} %add_rsqrt_fusion), kind=kOutput, calls=%fused_computation.30 | convolution fusion | flops 2955608064 | bytes 14033920 | tf_op jit(solution)/shard_map/dot_general | solution.py:114
  484.6 3.4 collective-permute-start
  487.9 0.0 copy-done.5
  488.0 1.6 collective-permute-done
  489.7 0.8 maximum_convert_fusion
  490.5 3.5 fusion.19
  493.9 165.6 %all-gather.14.cloned.1.call-done = bf16[2816,2048]{1,0:T(8,128)(2,1)} async-done(((bf16[2816,128]{1,0:T(8,128)(2,1)}), bf16[2816,2048]{1,0:T(8,128)(2,1)}) %all-gather.14.cloned.1.call-update) | async-done | bytes 11534352 | tf_op jit(solution)/shard_map/all_gather | solution.py:132
  659.5 10.4 %convolution_convert_fusion.2 = bf16[256,2048]{1,0:T(8,128)(2,1)} fusion(bf16[2816,2048]{1,0:T(8,128)(2,1)} %all-gather.14.cloned.1.call-done, f32[256,5632]{1,0:T(8,128)} %fusion.19), kind=kOutput, calls=%fused_computation.37 | convolution fusion | flops 2957639680 | bytes 18350080 | tf_op jit(solution)/shard_map/dot_general | solution.py:130
  669.9 0.0 reduce-scatter.2.cloned.1.call-update
  669.9 6.7 reduce-scatter.2.cloned.1.call-done
  676.6 0.0 copy-done.3
  676.6 2.0 add_convert_fusion
  (38 shorter events, 0.4 us)
Async XLA Ops:
  6.5 106.0 %copy-start = (bf16[1024,1024]{1,0:T(8,128)(2,1)S(1)}, bf16[1024,1024]{1,0:T(8,128)(2,1)}, u32[]{:S(2)}) copy-start(bf16[1024,1024]{1,0:T(8,128)(2,1)} %param.18) | copy-start | bytes 6291460
  6.5 93.6 %all-gather.6.cloned.1.call-start = ((), (), s32[]{:S(2)}) async-start(), calls=%async_computation.1 | async-start | bytes 4456448 | tf_op jit(solution)/shard_map/all_gather | solution.py:62
  8.5 180.6 %all-gather.8.cloned.1.call-start = ((), (), s32[]{:S(2)}) async-start(), calls=%async_computation.2 | async-start | bytes 1572864 | tf_op jit(solution)/shard_map/all_gather | solution.py:106
  100.2 12.4 %copy-start.4 = (bf16[256,1024]{1,0:T(8,128)(2,1)S(1)}, bf16[256,1024]{1,0:T(8,128)(2,1)}, u32[]{:S(2)}) copy-start(bf16[256,1024]{1,0:T(8,128)(2,1)} %param.14) | copy-start | bytes 1572868
  103.0 2.0 copy-start.2
  110.4 224.1 %copy-start.6 = (f32[2048]{0:T(1024)S(1)}, f32[2048]{0:T(1024)}, u32[]{:S(2)}) copy-start(f32[2048]{0:T(1024)} %param.19) | copy-start | bytes 24580
  114.1 220.3 %all-gather.10.cloned.1.call-start = ((), (), s32[]{:S(2)}) async-start(), calls=%async_computation.3 | async-start | bytes 12255232 | tf_op jit(solution)/shard_map/all_gather | solution.py:111
  114.9 361.8 %all-gather.12.cloned.1.call-start = ((), (), s32[]{:S(2)}) async-start(), calls=%async_computation.4 | async-start | bytes 12255232 | tf_op jit(solution)/shard_map/all_gather | solution.py:116
  115.4 544.1 %all-gather.14.cloned.1.call-start = ((), (), s32[]{:S(2)}) async-start(), calls=%async_computation.5 | async-start | bytes 12255232 | tf_op jit(solution)/shard_map/all_gather | solution.py:132
  116.0 560.6 %reduce-scatter.2.cloned.1.call-start = ((), (), s32[]{:S(2)}) async-start(), calls=%async_computation.6 | async-start | bytes 1572864 | tf_op jit(solution)/shard_map/reduce_scatter | solution.py:135
  342.3 145.6 %copy-start.5 = (f32[3,2,2816]{2,1,0:T(2,128)S(1)}, f32[3,2,2816]{2,1,0:T(2,128)}, u32[]{:S(2)}) copy-start(f32[3,2,2816]{2,1,0:T(2,128)} %param.22) | copy-start | bytes 202756
  484.6 5.1 collective-permute-start
  493.9 182.7 %copy-start.3 = (bf16[256,1024]{1,0:T(8,128)(2,1)S(1)}, bf16[256,1024]{1,0:T(8,128)(2,1)}, u32[]{:S(2)}) copy-start(bf16[256,1024]{1,0:T(8,128)(2,1)} %fusion.27) | copy-start | bytes 1572868
  659.5 19.2 %copy-start.1 = (bf16[1024,1024]{1,0:T(8,128)(2,1)S(1)}, bf16[1024,1024]{1,0:T(8,128)(2,1)}, u32[]{:S(2)}) copy-start(bf16[1024,1024]{1,0:T(8,128)(2,1)} %param.18) | copy-start | bytes 6291460
Sparse Core Ops, SparseCore 0:
  10.1 90.0 all-gather.5
  114.2 74.7 all-gather.7
  191.8 142.5 all-gather.9
  337.1 139.5 all-gather.11
  479.3 180.2 all-gather.13
  670.0 6.5 reduce-scatter.1
where the time goes:
time: 686 us
  waiting for transfers between devices  573 us (84%)
  blocking collectives  45.8 us (7%)
  matrix products  33.4 us (5%)
  between operations  13.6 us (2%)
  other arithmetic  9.58 us (1%)
    all_gather x1, waiting for transfers between devices, local(): lax.all_gather(down_weight, 'sp', axis=1, tiled=True)  166 us
    all_gather x1, waiting for transfers between devices, local(): lax.all_gather(gate_weight, 'sp', axis=0, tiled=True)  144 us
    all_gather x1, waiting for transfers between devices, local(): lax.all_gather(up_weight, 'sp', axis=0, tiled=True)  134 us
    all_gather x1, waiting for transfers between devices, local(): lax.all_gather(middle, 'tp', axis=1, tiled=True).astype(jnp.float32)  73 us
    all_gather x1, waiting for transfers between devices, attend(): arrived = lax.all_gather(keys_values, 'sp', axis=1, tiled=True)  46.1 us
    all_gather x1, blocking collectives, attend(): all_gates = lax.all_gather(cum_gate, 'sp', axis=1, tiled=True)  43.6 us
  transfers between devices with their start and end apart: 7, of which 7 were waited for; matrix products, arithmetic and copies ran while one was open for 3% of the time, Pallas kernels for 0%

commit v1 on v0

--- a/solution.py
+++ b/solution.py
@@ -129,7 +129,7 @@
     hidden = (jax.nn.silu(mixed[:, :hidden_cols]) * mixed[:, hidden_cols:]).astype(jnp.bfloat16)
     partials = jnp.dot(
         hidden,
-        lax.all_gather(down_weight, "sp", axis=1, tiled=True),
+        jnp.concatenate(lax.all_gather(down_weight, "sp"), axis=1),
         preferred_element_type=jnp.float32,
     )
     channel_out = lax.psum_scatter(

time: 686 us -> 662 us (0.965)
  waiting for transfers between devices: 573 us -> 537 us
  local copies, waits for them, and re-layouts: 5.91 us -> 20.9 us
    all_gather x1, waiting for transfers between devices: 166 us -> 131 us  [local(): lax.all_gather(down_weight, 'sp')]
    reshape x0 -> x1, local copies, waits for them, and re-layouts: none -> 15 us  [local(): jnp.concatenate(lax.all_gather(down_weight, 'sp'), axis=1)]
    all_gather x1, waiting for transfers between devices: 144 us -> 134 us  [local(): lax.all_gather(gate_weight, 'sp', axis=0, tiled=True)]
    all_gather x1, waiting for transfers between devices: 134 us -> 144 us  [local(): lax.all_gather(up_weight, 'sp', axis=0, tiled=True)]
  transfers between devices with their start and end apart: 7 -> 7, of which waited for: 7 -> 6; matrix products, arithmetic and copies ran while one was open for 3% -> 5% of each run, Pallas kernels for 0% -> 0%
where the time goes in v1:
time: 662 us; the launch traced here: 661 us
  waiting for transfers between devices  537 us (81%)
  blocking collectives  45.8 us (7%)
  matrix products  31.7 us (5%)
  local copies, waits for them, and re-layouts  20.9 us (3%)
  between operations  13.7 us (2%)
  other arithmetic  7.84 us (1%)
    all_gather x1, waiting for transfers between devices, local(): lax.all_gather(up_weight, 'sp', axis=0, tiled=True)  144 us
    all_gather x1, waiting for transfers between devices, local(): lax.all_gather(gate_weight, 'sp', axis=0, tiled=True)  134 us
    all_gather x1, waiting for transfers between devices, local(): lax.all_gather(down_weight, 'sp')  131 us
    all_gather x1, waiting for transfers between devices, local(): lax.all_gather(middle, 'tp', axis=1, tiled=True).astype(jnp.float32)  72.7 us
    all_gather x1, waiting for transfers between devices, attend(): arrived = lax.all_gather(keys_values, 'sp', axis=1, tiled=True)  46.1 us
    all_gather x1, blocking collectives, attend(): all_gates = lax.all_gather(cum_gate, 'sp', axis=1, tiled=True)  43.6 us
    reshape x1, local copies, waits for them, and re-layouts, local(): jnp.concatenate(lax.all_gather(down_weight, 'sp'), axis=1)  15 us
  transfers between devices with their start and end apart: 7, of which 6 were waited for; matrix products, arithmetic and copies ran while one was open for 5% of the time, Pallas kernels for 0%

profile of v1, /device:TPU:0, one launch (start us, length us, event | category | flops | bytes accessed | tf_op | source)
XLA Modules:
  0.0 660.8 jit_solution(4545531902259402513)
XLA Ops:
  6.5 0.0 all-gather.7.cloned.1.call-start
  6.5 1.9 copy.18
  8.5 0.0 all-gather.7.cloned.1.call-update
  8.5 0.0 all-gather.9.cloned.1.call-start
  8.6 1.8 copy.19
  10.4 43.6 %all_gather.25 = f32[8,4096]{1,0:T(8,128)S(1)} all-gather(f32[8,256]{1,0:T(8,128)} %param.17), channel_id=1, replica_groups=mesh['sp'=16,'tp'=2] {'sp'}, dimensions={1}, use_global_device_ids=true | all-gather | bytes 139264 | tf_op jit(solution)/shard_map/all_gather | solution.py:23
  54.0 46.1 %all-gather.7.cloned.1.call-done = bf16[4,4096,128]{1,2,0:T(8,128)(2,1)} async-done(((bf16[4,256,128]{1,2,0:T(8,128)(2,1)}), bf16[4,4096,128]{1,2,0:T(8,128)(2,1)}) %all-gather.7.cloned.1.call-update) | async-done | bytes 4194320 | tf_op jit(solution)/shard_map/all_gather | solution.py:62
  100.2 0.0 copy-start.4
  100.2 10.1 %while.18 = (s32[]{:T(128)}, f32[4,2,256]{2,1,0:T(2,128)S(1)}, f32[4,2,256]{2,1,0:T(2,128)S(1)}, f32[4,2,256,64]{2,3,1,0:T(8,128)S(1)}, s32[]{:T(128)}, /*index=...) while((s32[]{:T(128)}, f32[4,2,256]{2,1,0:T(2,128)S(1)}, ...), condition=%wide.region_5.6_spmd.clone, body=%wide.region_0.5_spmd.clone.sunk | while | flops 288756480 | bytes 32014712 | solution.py:76
  100.3 9.6 %conditional.3 = ((f32[4,2,256]{2,1,0:T(2,128)S(1)}, f32[4,2,256]{2,1,0:T(2,128)S(1)}, f32[4,2,256,64]{2,3,1,0:T(8,128)S(1)})) conditional(s32[]{:T(128)} %convert_element_type.103, (f32[4,2,256]{2,1,0:T(2,128)S(1)}, f32[4,2,256]{2,1,0:T(2,128)S(1)}, f32[4,2,256,64]{2,3,1,0:T(8,128)S(1)}) %tuple.53, (s32[]{:T(128)}, s32[]{:T(128)}, ...), branch_computations={%region_1.0_spmd, %region_2.4_spmd} | conditional | flops 288756480 | bytes 32013442 | solution.py:69
  100.3 0.1 broadcast_compare_fusion
  100.5 2.4 fusion.6
  103.0 2.0 copy-done.2
  105.0 1.5 fusion.5
  106.5 3.4 fusion.10
  110.3 0.1 divide_convert_fusion
  110.3 0.0 copy-start.6
  110.4 2.2 all_gather.26
  112.5 0.0 copy-done
  112.5 1.5 fusion.27
  114.1 0.0 all-gather.9.cloned.1.call-update
  114.1 0.0 all-gather.13.cloned.1.call-start
  114.1 0.7 all-gather.13.cloned.1.call-update
  114.8 0.0 all-gather.11.cloned.1.call-start
  114.9 0.5 all-gather.11.cloned.1.call-update
  115.4 0.0 all-gather.15.cloned.1.call-start
  115.4 0.5 all-gather.15.cloned.1.call-update
  116.0 0.0 reduce-scatter.2.cloned.1.call-start
  116.0 72.7 %all-gather.9.cloned.1.call-done = bf16[256,2048]{1,0:T(8,128)(2,1)} async-done(((bf16[256,1024]{1,0:T(8,128)(2,1)}), bf16[256,2048]{1,0:T(8,128)(2,1)}) %all-gather.9.cloned.1.call-update) | async-done | bytes 1048592 | tf_op jit(solution)/shard_map/all_gather | solution.py:106
  188.8 1.5 fusion.22
  190.3 143.9 %all-gather.13.cloned.1.call-done = bf16[2048,2816]{1,0:T(8,128)(2,1)} async-done(((bf16[128,2816]{1,0:T(8,128)(2,1)}), bf16[2048,2816]{1,0:T(8,128)(2,1)}) %all-gather.13.cloned.1.call-update) | async-done | bytes 11534352 | tf_op jit(solution)/shard_map/all_gather | solution.py:116
  334.2 0.0 copy-done.6
  334.2 7.8 %convolution_convert_fusion = bf16[256,2816]{1,0:T(8,128)(2,1)S(1)} fusion(bf16[2048,2816]{1,0:T(8,128)(2,1)} %all-gather.13.cloned.1.call-done, bf16[256,2048]{1,0:T(8,128)(2,1)} %all-gather.9.cloned.1.call-done, f32[2048]{0:T(1024)S(1)} %copy-done.6, f32[256]{0:T(256)S(1)} %add_rsqrt_fusion), kind=kOutput, calls=%fused_computation.30 | convolution fusion | flops 2955608064 | bytes 14033920 | tf_op jit(solution)/shard_map/dot_general | solution.py:114
  342.0 0.0 copy-start.5
  342.0 134.4 %all-gather.11.cloned.1.call-done = bf16[2048,2816]{1,0:T(8,128)(2,1)} async-done(((bf16[128,2816]{1,0:T(8,128)(2,1)}), bf16[2048,2816]{1,0:T(8,128)(2,1)}) %all-gather.11.cloned.1.call-update) | async-done | bytes 11534352 | tf_op jit(solution)/shard_map/all_gather | solution.py:111
  476.4 7.8 %convolution_convert_fusion.1 = bf16[256,2816]{1,0:T(8,128)(2,1)S(1)} fusion(bf16[2048,2816]{1,0:T(8,128)(2,1)} %all-gather.11.cloned.1.call-done, bf16[256,2048]{1,0:T(8,128)(2,1)} %all-gather.9.cloned.1.call-done, f32[2048]{0:T(1024)S(1)} %copy-done.6, f32[256]{0:T(256)S(1)} %add_rsqrt_fusion), kind=kOutput, calls=%fused_computation.31 | convolution fusion | flops 2955608064 | bytes 14033920 | tf_op jit(solution)/shard_map/dot_general | solution.py:109
  484.3 3.4 collective-permute-start
  487.7 131.2 %all-gather.15.cloned.1.call-done = bf16[45056,128]{1,0:T(8,128)(2,1)} async-done(((bf16[2816,128]{1,0:T(8,128)(2,1)}), bf16[45056,128]{1,0:T(8,128)(2,1)}) %all-gather.15.cloned.1.call-update) | async-done | bytes 11534352 | tf_op jit(solution)/shard_map/all_gather | solution.py:132
  618.9 15.0 %copy.20 = bf16[2816,16,128]{0,2,1:T(8,128)(2,1)} copy(bf16[2816,16,128]{2,0,1:T(8,128)(2,1)} %bitcast.47) | data formatting | bytes 23068672 | tf_op jit(solution)/shard_map/reshape | solution.py:132
  633.9 0.0 collective-permute-done
  633.9 0.8 maximum_convert_fusion
  634.8 1.7 fusion.19
  636.5 0.0 copy-start.3
  636.5 0.0 copy-start.1
  636.5 8.7 %convolution_convert_fusion.2 = bf16[256,2048]{1,0:T(8,128)(2,1)} fusion(bf16[2816,2048]{0,1:T(8,128)(2,1)} %bitcast.48, f32[256,5632]{1,0:T(8,128)S(1)} %fusion.19), kind=kOutput, calls=%fused_computation.37 | convolution fusion | flops 2957639680 | bytes 18350080 | tf_op jit(solution)/shard_map/dot_general | solution.py:130
  645.2 0.0 reduce-scatter.2.cloned.1.call-update
  645.2 6.7 %reduce-scatter.2.cloned.1.call-done = bf16[256,1024]{1,0:T(8,128)(2,1)} async-done(((bf16[256,2048]{1,0:T(8,128)(2,1)}), bf16[256,1024]{1,0:T(8,128)(2,1)}) %reduce-scatter.2.cloned.1.call-update) | async-done | bytes 524304 | tf_op jit(solution)/shard_map/reduce_scatter | solution.py:135
  652.0 2.0 add_convert_fusion
  (39 shorter events, 0.3 us)
Async XLA Ops:
  6.5 106.0 %copy-start = (bf16[1024,1024]{1,0:T(8,128)(2,1)S(1)}, bf16[1024,1024]{1,0:T(8,128)(2,1)}, u32[]{:S(2)}) copy-start(bf16[1024,1024]{1,0:T(8,128)(2,1)} %param.18) | copy-start | bytes 6291460
  6.5 93.6 %all-gather.7.cloned.1.call-start = ((), (), s32[]{:S(2)}) async-start(), calls=%async_computation.1 | async-start | bytes 4456448 | tf_op jit(solution)/shard_map/all_gather | solution.py:62
  8.5 180.3 %all-gather.9.cloned.1.call-start = ((), (), s32[]{:S(2)}) async-start(), calls=%async_computation.2 | async-start | bytes 1572864 | tf_op jit(solution)/shard_map/all_gather | solution.py:106
  100.2 12.3 %copy-start.4 = (bf16[256,1024]{1,0:T(8,128)(2,1)S(1)}, bf16[256,1024]{1,0:T(8,128)(2,1)}, u32[]{:S(2)}) copy-start(bf16[256,1024]{1,0:T(8,128)(2,1)} %param.14) | copy-start | bytes 1572868
  103.0 2.0 copy-start.2
  110.3 223.8 %copy-start.6 = (f32[2048]{0:T(1024)S(1)}, f32[2048]{0:T(1024)}, u32[]{:S(2)}) copy-start(f32[2048]{0:T(1024)} %param.19) | copy-start | bytes 24580
  114.1 220.1 %all-gather.13.cloned.1.call-start = ((), (), s32[]{:S(2)}) async-start(), calls=%async_computation.4 | async-start | bytes 12255232 | tf_op jit(solution)/shard_map/all_gather | solution.py:116
  114.8 361.6 %all-gather.11.cloned.1.call-start = ((), (), s32[]{:S(2)}) async-start(), calls=%async_computation.3 | async-start | bytes 12255232 | tf_op jit(solution)/shard_map/all_gather | solution.py:111
  115.4 503.5 %all-gather.15.cloned.1.call-start = ((), (), s32[]{:S(2)}) async-start(), calls=%async_computation.6 | async-start | bytes 12255232 | tf_op jit(solution)/shard_map/all_gather | solution.py:132
  116.0 536.0 %reduce-scatter.2.cloned.1.call-start = ((), (), s32[]{:S(2)}) async-start(), calls=%async_computation.5 | async-start | bytes 1572864 | tf_op jit(solution)/shard_map/reduce_scatter | solution.py:135
  342.0 145.6 %copy-start.5 = (f32[3,2,2816]{2,1,0:T(2,128)S(1)}, f32[3,2,2816]{2,1,0:T(2,128)}, u32[]{:S(2)}) copy-start(f32[3,2,2816]{2,1,0:T(2,128)} %param.22) | copy-start | bytes 202756
  484.3 149.7 %collective-permute-start = (bf16[2,5632]{1,0:T(2,128)(2,1)S(1)}, bf16[2,5632]{1,0:T(2,128)(2,1)S(1)}, u32[]{:S(2)}, u32[]{:S(2)}) collective-permute-start(bf16[2,5632]{1,0:T(2,128)(2,1)S(1)} %pad_maximum_fusion), channel_id=1, source_target_pairs={{0,2},{2,4},{4,6},{6,8},{8,10},{10,12},{12,14},{14,16},{16,18},{18... | collective-permute-start | bytes 67592 | tf_op jit(solution)/shard_map/ppermute | solution.py:12
  636.5 15.5 %copy-start.3 = (bf16[256,1024]{1,0:T(8,128)(2,1)S(1)}, bf16[256,1024]{1,0:T(8,128)(2,1)}, u32[]{:S(2)}) copy-start(bf16[256,1024]{1,0:T(8,128)(2,1)} %fusion.27) | copy-start | bytes 1572868
  636.5 17.5 %copy-start.1 = (bf16[1024,1024]{1,0:T(8,128)(2,1)S(1)}, bf16[1024,1024]{1,0:T(8,128)(2,1)}, u32[]{:S(2)}) copy-start(bf16[1024,1024]{1,0:T(8,128)(2,1)} %param.18) | copy-start | bytes 6291460
Sparse Core Ops, SparseCore 0:
  10.1 90.0 all-gather.6
  114.2 74.5 all-gather.8
  191.5 142.5 all-gather.12
  336.8 139.5 all-gather.10
  479.0 139.8 all-gather.14
  645.4 6.5 reduce-scatter.1
